TPU v7x, 32 devices: a whole 2x2x4 slice. The times are simulated.
32 devices in a mesh: sp: 8 (over z, y), tp: 4 (over x, core).
Axes of the slice: x: 2, y: 2, z: 4, core: 2. Of those that a mesh axis runs over, the one named last changes fastest.
Arguments:
- tokens: bfloat16 [3072, 2048], P(('sp', 'tp')), may hold values from -60 to 60
- query_weight: bfloat16 [2048, 1024], P(None, 'tp'), may hold values from -0.125 to 0.125
- key_weight: bfloat16 [2048, 1024], P(None, 'tp'), may hold values from -0.125 to 0.125
- value_weight: bfloat16 [2048, 1024], P(None, 'tp'), may hold values from -0.125 to 0.125
- outer_gate: bfloat16 [2048, 1024], P(None, 'tp'), may hold values from -0.125 to 0.125
- inner_gate: bfloat16 [2048, 1024], P(None, 'tp'), may hold values from -0.125 to 0.125
- conv_weight: bfloat16 [2048, 1024], P(None, 'tp'), may hold values from -0.125 to 0.125
- conv_taps: bfloat16 [3, 1024], P(None, 'tp'), may hold values from -3 to 3
- gate_sum: float32 [8, 3072], P('tp'), may hold values from -180 to 0, as said below
- head_gain: bfloat16 [1024], P('tp'), may hold values from 0.099609375 to 1.8984375
- channel_gain: bfloat16 [1024], P('tp'), may hold values from 0.099609375 to 1.8984375
- attention_out: bfloat16 [1024, 2048], P('tp'), may hold values from -0.125 to 0.125
- channel_out: bfloat16 [1024, 2048], P('tp'), may hold values from -0.125 to 0.125
Outputs:
- mixed_out: bfloat16 [3072, 2048], P(('sp', 'tp'))
Inputs may be any that keep to these rules, and one draw needn't show every extreme that they name: gate_sum[h, t] never rises with t.
All inputs are finite; a program needn't handle non-finite values.
Results may differ from a plain program's by a relative error of at most 0.015.
Values may be sent and summed in bfloat16 or wider, within the bound.
A program may use at most 192 MiB of HBM per device.

v0:
```python
import jax
import jax.numpy as jnp
from jax import lax
from jax.sharding import PartitionSpec as P

HEAD = 128
KTAP = 3


def passed_along(shard, axis, by):
    peers = lax.axis_size(axis)
    pairs = [(i, i + by) for i in range(peers) if 0 <= i + by < peers]
    return lax.ppermute(shard, axis, pairs)


def head_norm(values, gain_vector):
    row_count = values.shape[0]
    shaped = values.reshape(row_count, -1, HEAD)
    shaped = shaped * lax.rsqrt(jnp.mean(shaped * shaped, axis=-1, keepdims=True) + 1e-06)
    return (shaped.reshape(row_count, -1) * gain_vector.astype(jnp.float32)).astype(jnp.bfloat16)


def block_size(total_rows, unit_rows):
    best_rows = unit_rows
    for factor in range(1, total_rows // unit_rows + 1):
        if total_rows // unit_rows % factor == 0 and factor * unit_rows <= 2048:
            best_rows = factor * unit_rows
    return best_rows


def local(
    tokens,
    query_weight,
    key_weight,
    value_weight,
    outer_gate,
    inner_gate,
    conv_weight,
    conv_taps,
    gate_sum,
    head_gain,
    channel_gain,
    attention_out,
    channel_out,
):
    weight_list = (query_weight, key_weight, value_weight, outer_gate, inner_gate, conv_weight)

    def project_rows(piece_rows):
        return jnp.concatenate(
            [
                jnp.dot(piece_rows, weight, preferred_element_type=jnp.float32).astype(jnp.bfloat16)
                for weight in weight_list
            ],
            axis=1,
        )

    projected = project_rows(lax.all_gather(tokens, "tp", axis=0, tiled=True))
    pieces_list = []
    offset = 0
    for weight in weight_list:
        pieces_list.append(projected[:, offset : offset + weight.shape[1]])
        offset = offset + weight.shape[1]
    queries, keys_here, values_here, gate_outer, gate_inner, conv_input = pieces_list
    row_count = projected.shape[0]
    first_row = lax.axis_index("sp") * row_count
    mixed_in = (gate_inner.astype(jnp.float32) * conv_input.astype(jnp.float32)).astype(
        jnp.bfloat16
    )
    carried = passed_along(mixed_in[row_count - (KTAP - 1) :], "sp", 1)
    padded = jnp.concatenate([carried, mixed_in], axis=0).astype(jnp.float32)
    summed = jnp.zeros(mixed_in.shape, jnp.float32)
    for offset in range(KTAP):
        summed = (
            summed + conv_taps[offset].astype(jnp.float32) * padded[offset : offset + row_count]
        )
    conv_out = gate_outer.astype(jnp.float32) * summed
    heads_here = queries.shape[1] // HEAD
    query_heads = queries.reshape(row_count, heads_here, HEAD)
    query_gate = lax.dynamic_slice_in_dim(gate_sum, first_row, row_count, 1).T
    query_pos = first_row + jnp.arange(row_count, dtype=jnp.int32)
    last_row = first_row + row_count - 1
    score_scale = HEAD ** (-0.5)
    initial = (
        jnp.full((row_count, heads_here), -jnp.inf, jnp.float32),
        jnp.zeros((row_count, heads_here), jnp.float32),
        jnp.zeros((row_count, heads_here, HEAD), jnp.float32),
    )
    key_piece = lax.all_gather(keys_here, "sp", axis=0, tiled=True)
    value_piece = lax.all_gather(values_here, "sp", axis=0, tiled=True)
    piece_length = key_piece.shape[0]
    span_rows = block_size(piece_length, row_count)

    def one_block(block_index, state_in):
        key_start = block_index * span_rows

        def work(state_old):
            peak_old, total_old, accum_old = state_old
            key_block = lax.dynamic_slice_in_dim(
                key_piece, block_index * span_rows, span_rows, 0
            ).reshape(span_rows, heads_here, HEAD)
            value_block = lax.dynamic_slice_in_dim(
                value_piece, block_index * span_rows, span_rows, 0
            ).reshape(span_rows, heads_here, HEAD)
            gate_block = lax.dynamic_slice_in_dim(gate_sum, key_start, span_rows, 1)
            logits = (
                jnp.einsum(
                    "qhd,khd->qhk", query_heads, key_block, preferred_element_type=jnp.float32
                )
                * score_scale
            )
            logits = logits + query_gate[:, :, None] - gate_block[None, :, :]
            key_pos = key_start + jnp.arange(span_rows, dtype=jnp.int32)
            allowed = (key_pos[None, :] <= query_pos[:, None])[:, None, :]
            peak_new = jnp.maximum(peak_old, jnp.max(jnp.where(allowed, logits, -jnp.inf), axis=-1))
            peak_safe = jnp.where(peak_new > -jnp.inf, peak_new, 0.0)
            weights = jnp.where(allowed, jnp.exp(logits - peak_safe[..., None]), 0.0)
            rescale = jnp.exp(peak_old - peak_safe)
            total_new = total_old * rescale + jnp.sum(weights, axis=-1)
            accum_new = accum_old * rescale[..., None] + jnp.einsum(
                "qhk,khd->qhd",
                weights.astype(jnp.bfloat16),
                value_block,
                preferred_element_type=jnp.float32,
            )
            return (peak_new, total_new, accum_new)

        return lax.cond(key_start <= last_row, work, lambda state_old: state_old, state_in)

    peak_end, total_end, accum_end = lax.fori_loop(0, piece_length // span_rows, one_block, initial)
    attention = (accum_end / total_end[..., None]).reshape(row_count, heads_here * HEAD)
    head_normed = head_norm(attention, head_gain)
    group_normed = head_norm(conv_out, channel_gain)
    return lax.psum_scatter(
        (
            jnp.dot(head_normed, attention_out, preferred_element_type=jnp.float32)
            + jnp.dot(group_normed, channel_out, preferred_element_type=jnp.float32)
        ).astype(jnp.bfloat16),
        "tp",
        scatter_dimension=0,
        tiled=True,
    )


def solution(mesh):
    placed = (
        P(("sp", "tp"), None),
        P(None, "tp"),
        P(None, "tp"),
        P(None, "tp"),
        P(None, "tp"),
        P(None, "tp"),
        P(None, "tp"),
        P(None, "tp"),
        P("tp", None),
        P("tp"),
        P("tp"),
        P("tp", None),
        P("tp", None),
    )
    return jax.shard_map(
        local, mesh=mesh, in_specs=placed, out_specs=P(("sp", "tp"), None), check_vma=False
    )
```

profile of v0, /device:TPU:25, one launch (start us, length us, event | category | flops | bytes accessed | tf_op | source)
XLA Modules:
  0.0 172.3 jit_solution(3127703102989891153)
XLA Ops:
  7.3 22.6 %all-gather.4.cloned.1.call-done = bf16[384,2048]{1,0:T(8,128)(2,1)} async-done(((bf16[96,2048]{1,0:T(8,128)(2,1)}), bf16[384,2048]{1,0:T(8,128)(2,1)}) %all-gather.4.cloned.1.call-update) | async-done | bytes 1572880 | tf_op jit(solution)/shard_map/all_gather | solution.py:57
  29.9 3.1 %convolution_convert_fusion.3 = bf16[384,256]{1,0:T(8,128)(2,1)} fusion(bf16[384,2048]{1,0:T(8,128)(2,1)} %all-gather.4.cloned.1.call-done, bf16[2048,256]{1,0:T(8,128)(2,1)} %param.20), kind=kOutput, calls=%fused_computation.32 | convolution fusion | flops 402751488 | bytes 2818048 | tf_op jit(solution)/shard_map/dot_general | solution.py:51
  33.1 2.5 %convolution_convert_fusion.5 = bf16[384,256]{1,0:T(8,128)(2,1)} fusion(bf16[384,2048]{1,0:T(8,128)(2,1)S(1)} %copy-done.1, bf16[2048,256]{1,0:T(8,128)(2,1)} %param.19), kind=kOutput, calls=%fused_computation.34 | convolution fusion | flops 402751488 | bytes 2818048 | tf_op jit(solution)/shard_map/dot_general | solution.py:51
  35.8 2.1 %fusion.19 = f32[384,256]{0,1:T(8,128)S(1)} fusion(bf16[384,2048]{1,0:T(8,128)(2,1)S(1)} %copy-done.1, bf16[2048,256]{1,0:T(8,128)(2,1)} %param.22), kind=kOutput, calls=%fused_computation.28 | convolution fusion | flops 402849792 | bytes 3014656 | tf_op jit(solution)/shard_map/dot_general | solution.py:51
  38.7 3.1 %collective-permute-start = (bf16[2,256]{0,1:T(8,128)(2,1)S(1)}, bf16[2,256]{0,1:T(8,128)(2,1)S(1)}, u32[]{:S(2)}, u32[]{:S(2)}) collective-permute-start(bf16[2,256]{0,1:T(8,128)(2,1)S(1)} %slice.28), channel_id=1, source_target_pairs={{0,4},{4,8},{8,12},{12,16},{16,20},{20,24},{24,28},{1,5},{5,9},{9,... | collective-permute-start | bytes 3080 | tf_op jit(solution)/shard_map/ppermute | solution.py:13
  42.8 4.9 %collective-permute-done = bf16[2,256]{0,1:T(8,128)(2,1)S(1)} collective-permute-done((bf16[2,256]{0,1:T(8,128)(2,1)S(1)}, bf16[2,256]{0,1:T(8,128)(2,1)S(1)}, u32[]{:S(2)}, u32[]{:S(2)}) %collective-permute-start) | collective-permute-done | bytes 1056 | tf_op jit(solution)/shard_map/ppermute | solution.py:13
  47.8 2.0 %bitcast_reduce_fusion = (f32[384,2]{0,1:T(2,128)S(1)}, f32[384,256]{0,1:T(8,128)S(1)}) fusion(f32[386,256]{0,1:T(8,128)S(1)} %maximum_convert_fusion, f32[256]{0:T(256)S(1)} %bitcast.51, f32[256]{0:T(256)S(1)} %bitcast.52, f32[256]{0:T(256)S(1)} %bitcast.50, bf16[384,2048]{1,0:T(8,128)(2,1)S(1)} %copy-done.1, bf16[2048,256]{1,0:T(8,128)(2,1)} %param.21), kind=kOutput, calls=%fused_computation.44 | convolution fusion | flops 403635456 | bytes 4200448 | tf_op jit(solution)/shard_map/dot_general | solution.py:51
  50.0 25.5 %all-gather.8.cloned.1.call-done = bf16[3072,256]{1,0:T(8,128)(2,1)} async-done(((bf16[384,256]{1,0:T(8,128)(2,1)}), bf16[3072,256]{1,0:T(8,128)(2,1)}) %all-gather.8.cloned.1.call-update) | async-done | bytes 1572880 | tf_op jit(solution)/shard_map/all_gather | solution.py:89
  75.5 1.7 copy.23
  77.2 43.0 %all-gather.6.cloned.1.call-done = bf16[3072,256]{1,0:T(8,128)(2,1)} async-done(((bf16[384,256]{1,0:T(8,128)(2,1)}), bf16[3072,256]{1,0:T(8,128)(2,1)}) %all-gather.6.cloned.1.call-update) | async-done | bytes 1572880 | tf_op jit(solution)/shard_map/all_gather | solution.py:88
  120.3 2.6 %copy.21 = bf16[3072,256]{0,1:T(8,128)(2,1)} copy(bf16[3072,256]{1,0:T(8,128)(2,1)} %all-gather.6.cloned.1.call-done) | data formatting | bytes 3145728
  122.9 11.0 %while.18 = (s32[]{:T(128)}, f32[384,2]{0,1:T(2,128)S(1)}, f32[384,2]{0,1:T(2,128)S(1)}, f32[384,2,128]{0,2,1:T(8,128)S(1)}, s32[]{:T(128)}, /*index=5*/bf16[307...) while((s32[]{:T(128)}, f32[384,2]{0,1:T(2,128)S(1)}, ...), condition=%wide.region_5.6_spmd.clone, body=%wide.region_0.5_spmd.clone.sunk | while | flops 617748864 | bytes 22327704 | solution.py:129
  122.9 5.4 %conditional.3 = ((f32[384,2]{0,1:T(2,128)S(1)}, f32[384,2]{0,1:T(2,128)S(1)}, f32[384,2,128]{0,2,1:T(8,128)S(1)})) conditional(s32[]{:T(128)} %convert_element_type.120, (f32[384,2]{0,1:T(2,128)S(1)}, f32[384,2]{0,1:T(2,128)S(1)}, f32[384,2,128]{0,2,1:T(8,128)S(1)}) %tuple.51, (s32[]{:T(128)}, s32[]{:T(128)}, s32[]{:T(128)}, ...), branch_computations={%region_1.0_spmd, %region_2.4_spmd} | conditional | flops 617748864 | bytes 22325888 | solution.py:127
  123.4 1.2 constant_dynamic-slice_fusion
  124.7 1.5 select_reduce_fusion
  126.2 0.9 fusion.4
  127.2 1.2 fusion.13
  128.4 5.5 %conditional.3 = ((f32[384,2]{0,1:T(2,128)S(1)}, f32[384,2]{0,1:T(2,128)S(1)}, f32[384,2,128]{0,2,1:T(8,128)S(1)})) conditional(s32[]{:T(128)} %convert_element_type.120, (f32[384,2]{0,1:T(2,128)S(1)}, f32[384,2]{0,1:T(2,128)S(1)}, f32[384,2,128]{0,2,1:T(8,128)S(1)}) %tuple.51, (s32[]{:T(128)}, s32[]{:T(128)}, s32[]{:T(128)}, ...), branch_computations={%region_1.0_spmd, %region_2.4_spmd} | conditional | flops 617748864 | bytes 22325888 | solution.py:127
  128.9 1.3 constant_dynamic-slice_fusion
  130.2 1.5 select_reduce_fusion
  131.7 0.9 fusion.4
  132.7 1.2 fusion.13
  135.4 1.8 %add_convert_fusion = bf16[384,2048]{1,0:T(8,128)(2,1)} fusion(f32[384,2048]{1,0:T(8,128)S(1)} %fusion.28, bf16[384,256]{0,1:T(8,128)(2,1)S(1)} %fusion.26, bf16[256,2048]{1,0:T(8,128)(2,1)S(1)} %copy-done.4), kind=kOutput, calls=%fused_computation.23 | convolution fusion | flops 404226048 | bytes 5963776 | tf_op jit(solution)/shard_map/dot_general | solution.py:136
  137.2 28.6 %reduce-scatter.2.cloned.1.call-done = bf16[96,2048]{1,0:T(8,128)(2,1)} async-done(((bf16[384,2048]{1,0:T(8,128)(2,1)}), bf16[96,2048]{1,0:T(8,128)(2,1)}) %reduce-scatter.2.cloned.1.call-update) | async-done | bytes 393232 | tf_op jit(solution)/shard_map/reduce_scatter | solution.py:133
  (61 shorter events, 5.3 us)
Async XLA Ops:
  6.5 127.6 %copy-start = (bf16[256,2048]{1,0:T(8,128)(2,1)S(1)}, bf16[256,2048]{1,0:T(8,128)(2,1)}, u32[]{:S(2)}) copy-start(bf16[256,2048]{1,0:T(8,128)(2,1)} %param.28) | copy-start | bytes 3145732
  6.5 23.4 %all-gather.4.cloned.1.call-start = ((), (), s32[]{:S(2)}) async-start(), calls=%async_computation.1 | async-start | bytes 1966080 | tf_op jit(solution)/shard_map/all_gather | solution.py:57
  7.3 68.2 %all-gather.8.cloned.1.call-start = ((), (), s32[]{:S(2)}) async-start(), calls=%async_computation.3 | async-start | bytes 1769472 | tf_op jit(solution)/shard_map/all_gather | solution.py:89
  29.9 3.2 %copy-start.1 = (bf16[384,2048]{1,0:T(8,128)(2,1)S(1)}, bf16[384,2048]{1,0:T(8,128)(2,1)}, u32[]{:S(2)}) copy-start(bf16[384,2048]{1,0:T(8,128)(2,1)} %all-gather.4.cloned.1.call-done) | copy-start | bytes 4718596
  33.0 2.7 %copy-start.7 = (bf16[256]{0:T(256)(128)(2,1)S(1)}, bf16[256]{0:T(256)(128)(2,1)}, u32[]{:S(2)}) copy-start(bf16[256]{0:T(256)(128)(2,1)} %param.26) | copy-start | bytes 1540
  33.0 2.7 %copy-start.8 = (bf16[256]{0:T(256)(128)(2,1)S(1)}, bf16[256]{0:T(256)(128)(2,1)}, u32[]{:S(2)}) copy-start(bf16[256]{0:T(256)(128)(2,1)} %param.27) | copy-start | bytes 1540
  33.0 2.7 %copy-start.5 = (f32[2,3072]{1,0:T(2,128)S(1)}, f32[2,3072]{1,0:T(2,128)}, u32[]{:S(2)}) copy-start(f32[2,3072]{1,0:T(2,128)} %param.25) | copy-start | bytes 73732
  33.0 2.7 %copy-start.6 = (bf16[3,256]{1,0:T(4,128)(2,1)S(1)}, bf16[3,256]{1,0:T(4,128)(2,1)}, u32[]{:S(2)}) copy-start(bf16[3,256]{1,0:T(4,128)(2,1)} %param.24) | copy-start | bytes 4612
  33.0 87.2 %all-gather.6.cloned.1.call-start = ((), (), s32[]{:S(2)}) async-start(), calls=%async_computation.2 | async-start | bytes 1769472 | tf_op jit(solution)/shard_map/all_gather | solution.py:88
  35.6 130.2 %reduce-scatter.2.cloned.1.call-start = ((), (), s32[]{:S(2)}) async-start(), calls=%async_computation.4 | async-start | bytes 1966080 | tf_op jit(solution)/shard_map/reduce_scatter | solution.py:133
  35.7 2.1 %copy-start.2 = (bf16[2048,256]{1,0:T(8,128)(2,1)S(1)}, bf16[2048,256]{1,0:T(8,128)(2,1)}, u32[]{:S(2)}) copy-start(bf16[2048,256]{1,0:T(8,128)(2,1)} %param.23) | copy-start | bytes 3145732
  37.8 4.0 %copy-start.3 = (bf16[2048,256]{1,0:T(8,128)(2,1)S(1)}, bf16[2048,256]{1,0:T(8,128)(2,1)}, u32[]{:S(2)}) copy-start(bf16[2048,256]{1,0:T(8,128)(2,1)} %param.18) | copy-start | bytes 3145732
  38.7 8.9 %collective-permute-start = (bf16[2,256]{0,1:T(8,128)(2,1)S(1)}, bf16[2,256]{0,1:T(8,128)(2,1)S(1)}, u32[]{:S(2)}, u32[]{:S(2)}) collective-permute-start(bf16[2,256]{0,1:T(8,128)(2,1)S(1)} %slice.28), channel_id=1, source_target_pairs={{0,4},{4,8},{8,12},{12,16},{16,20},{20,24},{24,28},{1,5},{5,9},{9,... | collective-permute-start | bytes 3080 | tf_op jit(solution)/shard_map/ppermute | solution.py:13
  134.1 1.2 copy-start.4
Sparse Core Ops, SparseCore 0:
  8.9 20.9 all-gather.3
  33.2 42.2 all-gather.7
  77.7 42.5 all-gather.5
  137.3 28.4 reduce-scatter.1
where the time goes:
time: 175 us; the launch traced here: 172 us
  waiting for transfers between devices  125 us (71%)
  matrix products  19 us (11%)
  between operations  13.4 us (8%)
  local copies, waits for them, and re-layouts  7.82 us (4%)
  starting transfers between devices  3.23 us (2%)
  other arithmetic  3.19 us (2%)
    all_gather x1, waiting for transfers between devices, local(): key_piece = lax.all_gather(keys_here, 'sp', axis=0, tiled=True)  43 us
    reduce_scatter x1, waiting for transfers between devices, local(): lax.psum_scatter((jnp.dot(head_normed, attention_out, preferred_element_t...  28.6 us
    all_gather x1, waiting for transfers between devices, local(): value_piece = lax.all_gather(values_here, 'sp', axis=0, tiled=True)  25.5 us
    all_gather x1, waiting for transfers between devices, local(): projected = project_rows(lax.all_gather(tokens, 'tp', axis=0, tiled=True))  22.6 us
    dot_general x6, matrix products, project_rows(): jnp.dot(piece_rows, weight, preferred_element_type=jnp.float32)  11.2 us
    unnamed x21, local copies, waits for them, and re-layouts  5.14 us
    ppermute x1, waiting for transfers between devices, passed_along(): return lax.ppermute(shard, axis, pairs)  4.88 us
  transfers between devices with their start and end apart: 5, of which 5 were waited for; matrix products, arithmetic and copies ran while one was open for 6% of the time, Pallas kernels for 0%

commit v1 on v0

v1 whole, which is shorter than its diff:
```python
import functools
import math

import jax
import jax.numpy as jnp
from jax import lax
from jax.experimental import pallas as pl
from jax.experimental.pallas import tpu as pltpu
from jax.sharding import PartitionSpec as P

HEAD = 128
KTAP = 3
HALO = 16
MESH = pl.DeviceIdType.MESH
F32 = jnp.float32
BF16 = jnp.bfloat16


def rms(values, gain):
    scale = lax.rsqrt(jnp.mean(values * values, axis=-1, keepdims=True) + 1e-06)
    return (values * scale * gain).astype(BF16)


def kernel(
    S,
    T,
    tokens,
    wq,
    wk,
    wv,
    wgo,
    wgi,
    wci,
    taps,
    gate,
    head_gain,
    channel_gain,
    wattn,
    wchan,
    out,
    tok,
    w,
    wo,
    kv,
    qbuf,
    stage_kv,
    stage_q,
    gates,
    mixed,
    halo,
    padded,
    group,
    peak,
    total,
    acc,
    ret,
    heads,
    part,
    part_in,
    xsum,
    xsum_in,
    w_sem,
    wo_sem,
    tok_sem,
    tok_send,
    tok_recv,
    y_send,
    y_recv,
    kv_send,
    kv_far,
    kv_recv,
    halo_send,
    halo_recv,
    ret_send,
    ret_recv,
    pair_send,
    pair_recv,
    x_send,
    x_recv,
):
    sp = lax.axis_index("sp")
    tp = lax.axis_index("tp")
    G = S // 2
    g = sp // 2
    par = sp % 2
    mate = sp + 1 - 2 * par
    C = tokens.shape[0]
    R = C * T
    HR = R // 2
    R2 = 2 * R
    pair = tp // 2
    tp1 = tp + 1 - 2 * (tp % 2)
    tp2 = (tp + 2) % T
    tp3 = (tp1 + 2) % T
    near = G // 2

    weights = (wk, wv, wq, wgi, wci, wgo)
    own_copy = pltpu.make_async_copy(tokens, tok.at[pl.ds(tp * C, C)], tok_sem)
    own_copy.start()
    w_copies = [pltpu.make_async_copy(weights[i], w.at[i], w_sem.at[i]) for i in range(6)]
    for copy in w_copies:
        copy.start()
    wo_copies = [
        pltpu.make_async_copy(ref, wo.at[i], wo_sem.at[i]) for i, ref in enumerate((wattn, wchan))
    ]
    for copy in wo_copies:
        copy.start()

    barrier = pltpu.get_barrier_semaphore()
    for o in range(1, T):
        pl.semaphore_signal(barrier, inc=1, device_id={"tp": (tp + o) % T}, device_id_type=MESH)
    for o in range(1, S):
        pl.semaphore_signal(barrier, inc=1, device_id={"sp": (sp + o) % S}, device_id_type=MESH)
    pl.semaphore_wait(barrier, S + T - 2)

    def tok_copy(slot, target, index):
        rows = pl.ds(slot * C, C)
        return pltpu.make_async_remote_copy(
            src_ref=tok.at[rows],
            dst_ref=tok.at[rows],
            send_sem=tok_send.at[index],
            recv_sem=tok_recv.at[index],
            device_id={"tp": target},
            device_id_type=MESH,
        )

    own_copy.wait()
    cross = tok_copy(tp, tp2, 0)
    cross.start()
    beside = tok_copy(tp, tp1, 1)
    beside.start()

    def half_start(half):
        return (pair if half == 0 else 1 - pair) * HR

    def y_kv(half):
        rs = half_start(half)
        return pltpu.make_async_remote_copy(
            src_ref=stage_kv.at[:, pl.ds(rs, HR), :],
            dst_ref=kv.at[g, :, pl.ds(par * R + rs, HR), :],
            send_sem=y_send.at[half, 0],
            recv_sem=y_recv.at[half, 0],
            device_id={"sp": mate},
            device_id_type=MESH,
        )

    def y_q(half):
        rs = half_start(half)
        return pltpu.make_async_remote_copy(
            src_ref=stage_q.at[pl.ds(rs, HR), :],
            dst_ref=qbuf.at[pl.ds(par * R + rs, HR), :],
            send_sem=y_send.at[half, 1],
            recv_sem=y_recv.at[half, 1],
            device_id={"sp": mate},
            device_id_type=MESH,
        )

    def piece_copy(d, p, step, send_sem):
        half, other = p // 2, p % 2
        rows = pl.ds((1 - par if other else par) * R + half_start(half), HR)
        ref = kv.at[g - d, :, rows, :]
        return pltpu.make_async_remote_copy(
            src_ref=ref,
            dst_ref=ref,
            send_sem=send_sem,
            recv_sem=kv_recv.at[d + step, p],
            device_id={"sp": lax.rem(sp + 2 * step, S)},
            device_id_type=MESH,
        )

    def send_own(p):
        @pl.when(g + 1 < G)
        def _():
            piece_copy(0, p, 1, kv_send.at[0, p]).start()

        for step in range(near + 1, G):

            @pl.when(g + step < G)
            def _():
                piece_copy(0, p, step, kv_far.at[step, p]).start()

    def project(half, index):
        rs = pl.multiple_of(half_start(half), 16)
        rows = tok[pl.ds(rs, HR), :]
        return rs, jnp.dot(rows, w[index], preferred_element_type=F32).astype(BF16)

    def split(value):
        a, b = value[:, :HEAD], value[:, HEAD:]
        return jnp.where(par == 0, a, b), jnp.where(par == 0, b, a)

    def attention_inputs(half):
        for i in range(2):
            if half == 0:
                w_copies[i].wait()
            rs, value = project(half, i)
            mine, theirs = split(value)
            kv[g, i, pl.ds(pl.multiple_of(par * R + rs, 16), HR), :] = mine
            stage_kv[i, pl.ds(rs, HR), :] = theirs
        y_kv(half).start()
        send_own(2 * half)
        if half == 0:
            w_copies[2].wait()
        rs, value = project(half, 2)
        mine, theirs = split(value)
        qbuf[pl.ds(pl.multiple_of(par * R + rs, 16), HR), :] = mine
        stage_q[pl.ds(rs, HR), :] = theirs
        y_q(half).start()

    def gate_inputs(half):
        for i in range(3, 6):
            if half == 0:
                w_copies[i].wait()
            rs, value = project(half, i)
            gates[i - 3, pl.ds(rs, HR), :] = value

    beside.wait_recv()
    attention_inputs(0)
    gate_inputs(0)
    y_kv(0).wait_recv()
    send_own(1)

    tok_copy(tp2, tp2, 0).wait_recv()
    onward = tok_copy(tp2, tp1, 2)
    onward.start()
    tok_copy(tp3, tp1, 2).wait_recv()
    attention_inputs(1)
    gate_inputs(1)
    y_kv(1).wait_recv()
    send_own(3)

    mixed[...] = (gates[0].astype(F32) * gates[1].astype(F32)).astype(BF16)
    halo_copy = pltpu.make_async_remote_copy(
        src_ref=mixed.at[pl.ds(R - HALO, HALO), :],
        dst_ref=halo,
        send_sem=halo_send,
        recv_sem=halo_recv,
        device_id={"sp": lax.rem(sp + 1, S)},
        device_id_type=MESH,
    )

    @pl.when(sp + 1 < S)
    def _():
        halo_copy.start()

    y_q(0).wait_recv()
    y_q(1).wait_recv()

    log2e = math.log2(math.e)
    coefficient = log2e * HEAD ** (-0.5)
    QT = 256 if R2 % 256 == 0 else 128

    def attend(b, diagonal):
        bias = gate[pl.ds(par, 1), pl.ds(pl.multiple_of(b * R2, 128), R2)] * log2e
        for start in range(0, R2, QT):
            stop = start + QT if diagonal else R2
            rows = pl.ds(start, QT)
            s = lax.dot_general(
                qbuf[rows, :],
                kv[b, 0, pl.ds(0, stop), :],
                (((1,), (1,)), ((), ())),
                preferred_element_type=F32,
            )
            s = s * coefficient - bias[:, :stop]
            if diagonal:
                row = lax.broadcasted_iota(jnp.int32, s.shape, 0) + start
                col = lax.broadcasted_iota(jnp.int32, s.shape, 1)
                s = jnp.where(col <= row, s, -jnp.inf)
                top = jnp.max(s, axis=-1, keepdims=True)
            else:
                before = peak[rows, :]
                top = jnp.maximum(before, jnp.max(s, axis=-1, keepdims=True))
            weight = jnp.exp2(s - top)
            norm = jnp.sum(weight, axis=-1, keepdims=True)
            value = jnp.dot(
                weight.astype(BF16), kv[b, 1, pl.ds(0, stop), :], preferred_element_type=F32
            )
            if not diagonal:
                fade = jnp.exp2(before - top)
                norm = norm + total[rows, :] * fade
                value = value + acc[rows, :] * fade
            peak[rows, :] = top
            total[rows, :] = norm
            acc[rows, :] = value

    attend(g, True)

    @pl.when(sp > 0)
    def _():
        halo_copy.wait_recv()
        padded[0:8, :] = halo[HALO - 8 : HALO, :].astype(F32)

    @pl.when(sp == 0)
    def _():
        padded[0:8, :] = jnp.zeros((8, padded.shape[1]), F32)

    padded[pl.ds(8, R), :] = mixed[...].astype(F32)
    summed = jnp.zeros(mixed.shape, F32)
    for j in range(KTAP):
        summed = summed + taps[j : j + 1, :].astype(F32) * padded[pl.ds(9 - KTAP + j, R), :]
    conv_out = gates[2].astype(F32) * summed
    for h in range(conv_out.shape[1] // HEAD):
        cols = slice(h * HEAD, (h + 1) * HEAD)
        group[:, cols] = rms(conv_out[:, cols], channel_gain[:, cols].astype(F32))

    def chain(d, carry):
        for p in range(4):
            piece_copy(d - 1, p, 1, kv_send.at[0, p]).wait_recv()

            @pl.when((d < near) & (g + 1 < G))
            def _():
                piece_copy(d, p, 1, kv_send.at[d, p]).start()

        attend(g - d, False)
        return carry

    lax.fori_loop(1, g + 1, chain, 0)

    gain = jnp.where(par == 0, head_gain[:, :HEAD], head_gain[:, HEAD:]).astype(F32)

    def finished(first):
        rows = pl.ds(pl.multiple_of(first, 16), R)
        return rms(acc[rows, :] / total[rows, :], gain)

    ret[...] = finished((1 - par) * R)
    back = pltpu.make_async_remote_copy(
        src_ref=ret,
        dst_ref=heads.at[par],
        send_sem=ret_send,
        recv_sem=ret_recv,
        device_id={"sp": mate},
        device_id_type=MESH,
    )
    back.start()
    heads[par] = finished(par * R)
    for copy in wo_copies:
        copy.wait()
    back.wait_recv()

    NH = out.shape[1] // 2

    def partial(chunk, n):
        rows = pl.ds(pl.multiple_of(chunk * C, 16), C)
        both = jnp.concatenate([heads[0, rows, :], heads[1, rows, :]], axis=1)
        cols = pl.ds(n * NH, NH)
        return jnp.dot(both, wo[0, :, cols], preferred_element_type=F32) + jnp.dot(
            group[rows, :], wo[1, :, cols], preferred_element_type=F32
        )

    def pair_copy(i, n):
        return pltpu.make_async_remote_copy(
            src_ref=part.at[i, n],
            dst_ref=part_in.at[i, n],
            send_sem=pair_send.at[i, n],
            recv_sem=pair_recv.at[i, n],
            device_id={"tp": tp1},
            device_id_type=MESH,
        )

    def x_copy(n):
        return pltpu.make_async_remote_copy(
            src_ref=xsum.at[n],
            dst_ref=xsum_in.at[n],
            send_sem=x_send.at[n],
            recv_sem=x_recv.at[n],
            device_id={"tp": tp2},
            device_id_type=MESH,
        )

    for n in range(2):
        part[0, n] = partial(tp3, n).astype(BF16)
        pair_copy(0, n).start()
    for n in range(2):
        value = partial(tp2, n)
        pair_copy(0, n).wait_recv()
        xsum[n] = (value + part_in[0, n].astype(F32)).astype(BF16)
        x_copy(n).start()
    for n in range(2):
        part[1, n] = partial(tp1, n).astype(BF16)
        pair_copy(1, n).start()
    for n in range(2):
        value = partial(tp, n)
        pair_copy(1, n).wait_recv()
        value = value + part_in[1, n].astype(F32)
        x_copy(n).wait_recv()
        out[:, pl.ds(n * NH, NH)] = (value + xsum_in[n].astype(F32)).astype(BF16)

    cross.wait_send()
    beside.wait_send()
    onward.wait_send()
    for half in range(2):
        y_kv(half).wait_send()
        y_q(half).wait_send()
    back.wait_send()

    @pl.when(sp + 1 < S)
    def _():
        halo_copy.wait_send()

    for n in range(2):
        x_copy(n).wait_send()
        for i in range(2):
            pair_copy(i, n).wait_send()
    for p in range(4):

        @pl.when(g + 1 < G)
        def _():
            piece_copy(0, p, 1, kv_send.at[0, p]).wait_send()

        for d in range(1, near):

            @pl.when((g + 1 < G) & (g >= d))
            def _():
                piece_copy(d, p, 1, kv_send.at[d, p]).wait_send()

        for step in range(near + 1, G):

            @pl.when(g + step < G)
            def _():
                piece_copy(0, p, step, kv_far.at[step, p]).wait_send()


def local(S, T, tokens, *rest):
    (wq, wk, wv, wgo, wgi, wci, taps, gate, head_gain, channel_gain, wattn, wchan) = rest
    C, D = tokens.shape
    R = C * T
    A = wq.shape[1]
    G = S // 2
    N = wattn.shape[1]
    hbm = pl.BlockSpec(memory_space=pl.ANY)
    vmem = pl.BlockSpec(memory_space=pltpu.VMEM)
    dma = pltpu.SemaphoreType.DMA
    return pl.pallas_call(
        functools.partial(kernel, S, T),
        out_shape=jax.ShapeDtypeStruct((C, N), BF16),
        in_specs=[hbm] * 7 + [vmem] * 4 + [hbm] * 2,
        out_specs=vmem,
        scratch_shapes=[
            pltpu.VMEM((R, D), BF16),
            pltpu.VMEM((6, D, A), BF16),
            pltpu.VMEM((2, A, N), BF16),
            pltpu.VMEM((G, 2, 2 * R, HEAD), BF16),
            pltpu.VMEM((2 * R, HEAD), BF16),
            pltpu.VMEM((2, R, HEAD), BF16),
            pltpu.VMEM((R, HEAD), BF16),
            pltpu.VMEM((3, R, A), BF16),
            pltpu.VMEM((R, A), BF16),
            pltpu.VMEM((HALO, A), BF16),
            pltpu.VMEM((R + 8, A), F32),
            pltpu.VMEM((R, A), BF16),
            pltpu.VMEM((2 * R, 1), F32),
            pltpu.VMEM((2 * R, 1), F32),
            pltpu.VMEM((2 * R, HEAD), F32),
            pltpu.VMEM((R, HEAD), BF16),
            pltpu.VMEM((2, R, HEAD), BF16),
            pltpu.VMEM((2, 2, C, N // 2), BF16),
            pltpu.VMEM((2, 2, C, N // 2), BF16),
            pltpu.VMEM((2, C, N // 2), BF16),
            pltpu.VMEM((2, C, N // 2), BF16),
            dma((6,)),
            dma((2,)),
            dma,
            dma((3,)),
            dma((3,)),
            dma((2, 2)),
            dma((2, 2)),
            dma((G, 4)),
            dma((G, 4)),
            dma((G + 1, 4)),
            dma,
            dma,
            dma,
            dma,
            dma((2, 2)),
            dma((2, 2)),
            dma((2,)),
            dma((2,)),
        ],
        compiler_params=pltpu.CompilerParams(
            collective_id=0, has_side_effects=True, vmem_limit_bytes=60 * 1024 * 1024
        ),
    )(
        tokens,
        wq,
        wk,
        wv,
        wgo,
        wgi,
        wci,
        taps,
        gate,
        head_gain.reshape(1, A),
        channel_gain.reshape(1, A),
        wattn,
        wchan,
    )


def solution(mesh):
    S, T = mesh.shape["sp"], mesh.shape["tp"]
    cols = P(None, "tp")
    rows = P("tp", None)
    placed = (
        (P(("sp", "tp"), None),) + (cols,) * 7 + (rows, P("tp"), P("tp")) + (rows, rows)
    )
    return jax.shard_map(
        functools.partial(local, S, T),
        mesh=mesh,
        in_specs=placed,
        out_specs=P(("sp", "tp"), None),
        check_vma=False,
    )
```

time: 175 us -> 60.3 us (0.34); the launches traced: 172 us -> 60.1 us
  waiting for transfers between devices: 125 us -> 0 us
  Pallas kernels: 0 us -> 56.5 us
  matrix products: 19 us -> 0 us
  between operations: 13.4 us -> 0.01 us
  local copies, waits for them, and re-layouts: 7.82 us -> 3.55 us
  starting transfers between devices: 3.23 us -> 0 us
  other arithmetic: 3.19 us -> 0 us
    all_gather x3 -> x0, waiting for transfers between devices: 91.2 us -> none  [the longest x1 43 us: local(): key_piece = lax.all_gather(keys_here, 'sp', axis=0, tiled=True)]
    pallas_call x0 -> x1, Pallas kernels: none -> 56.5 us  [local(): pl.pallas_call(functools.partial(kernel, S, T), out_shape=jax.ShapeDtypeS...]
    reduce_scatter x1 -> x0, waiting for transfers between devices: 28.6 us -> none  [local(): lax.psum_scatter((jnp.dot(head_normed, attention_out, preferred_element_t...]
    dot_general x12 -> x0, matrix products: 19 us -> none  [the longest x6 11.2 us: project_rows(): jnp.dot(piece_rows, weight, preferred_element_type=jnp.float32)]
    ppermute x1 -> x0, waiting for transfers between devices: 4.88 us -> none  [passed_along(): return lax.ppermute(shard, axis, pairs)]
    unnamed x21 -> x3, local copies, waits for them, and re-layouts: 5.14 us -> 1.77 us
    ppermute x1 -> x0, starting transfers between devices: 3.11 us -> none  [passed_along(): return lax.ppermute(shard, axis, pairs)]
    dynamic_slice x4 -> x0, local copies, waits for them, and re-layouts: 2.54 us -> none  [the longest x2 2.52 us: work(): lax.dynamic_slice_in_dim(value_piece, block_index * span_rows, span_rows, 0)]
  transfers between devices with their start and end apart: 5 -> 0, of which waited for: 5 -> 0; matrix products, arithmetic and copies ran while one was open for 6% -> 0% of each run, Pallas kernels for 0% -> 0%
where the time goes in v1:
time: 60.3 us; the launch traced here: 60.1 us
  Pallas kernels  56.5 us (94%)
  local copies, waits for them, and re-layouts  3.55 us (6%)
    pallas_call x1, Pallas kernels, local(): pl.pallas_call(functools.partial(kernel, S, T), out_shape=jax.ShapeDtypeS...  56.5 us
    unnamed x3, local copies, waits for them, and re-layouts  1.77 us
    reshape x1, local copies, waits for them, and re-layouts, local(): head_gain.reshape(1, A)  1.23 us

profile of v1, /device:TPU:25, one launch (start us, length us, event | category | flops | bytes accessed | tf_op | source)
XLA Modules:
  0.0 60.1 jit_solution(16659588075402294444)
XLA Ops:
  0.0 0.0 copy-start
  0.0 1.2 %reshape.6.head_gain = bf16[1,256]{1,0:T(2,128)(2,1)} reshape(bf16[256]{0:T(256)(128)(2,1)} %param.22) | data formatting | bytes 1024 | tf_op jit(solution)/shard_map/reshape | solution.py:491
  1.2 0.0 copy-done
  1.2 0.5 reshape.7.channel_gain
  1.8 56.5 %shard_map.127 = bf16[96,2048]{1,0:T(8,128)(2,1)} custom-call(bf16[96,2048]{1,0:T(8,128)(2,1)} %tokens.1, bf16[2048,256]{1,0:T(8,128)(2,1)} %wq.1, bf16[2048,256]{1,0:T(8,128)(2,1)} %wk.1, bf16[2048,256]{1,0:T(8,128)(2,1)} %wv.1, bf16[2048,256]{1,0:T(8,128)(2,1)} %wgo.1, bf16[2048,256]{1,0:T(8,128)(2,1)} %wgi.1, bf16[2048,256]{1,0:T(8,128)(2,1)} %wci.1, ...), custom_call_target="tpu_custom_call" | custom-call | tf_op jit(solution)/shard_map/pallas_call | solution.py:432
  58.3 1.8 %copy.15 = bf16[96,2048]{1,0:T(8,128)(2,1)} copy(bf16[96,2048]{1,0:T(8,128)(2,1)} %shard_map.127) | data formatting | bytes 786432
Async XLA Ops:
  0.0 1.2 %copy-start = (bf16[256]{0:T(256)(128)(2,1)S(1)}, bf16[256]{0:T(256)(128)(2,1)}, u32[]{:S(2)}) copy-start(bf16[256]{0:T(256)(128)(2,1)} %param.23) | copy-start | bytes 1540

commit v2 on v1

--- a/solution.py
+++ b/solution.py
@@ -98,13 +98,11 @@
     own_copy = pltpu.make_async_copy(tokens, tok.at[pl.ds(tp * C, C)], tok_sem)
     own_copy.start()
     w_copies = [pltpu.make_async_copy(weights[i], w.at[i], w_sem.at[i]) for i in range(6)]
-    for copy in w_copies:
+    for copy in w_copies[:3]:
         copy.start()
     wo_copies = [
         pltpu.make_async_copy(ref, wo.at[i], wo_sem.at[i]) for i, ref in enumerate((wattn, wchan))
     ]
-    for copy in wo_copies:
-        copy.start()
 
     barrier = pltpu.get_barrier_semaphore()
     for o in range(1, T):
@@ -129,6 +127,8 @@
     cross.start()
     beside = tok_copy(tp, tp1, 1)
     beside.start()
+    for copy in w_copies[3:] + wo_copies:
+        copy.start()
 
     def half_start(half):
         return (pair if half == 0 else 1 - pair) * HR
@@ -178,6 +178,18 @@
             @pl.when(g + step < G)
             def _():
                 piece_copy(0, p, step, kv_far.at[step, p]).start()
+
+    def arrived(d, p, send_on):
+        piece_copy(d, p, 0, kv_send.at[d, p]).wait_recv()
+
+        @pl.when(jnp.logical_and(send_on, g + 1 < G))
+        def _():
+            piece_copy(d, p, 1, kv_send.at[d, p]).start()
+
+    def arrived_near(p):
+        @pl.when(g > 0)
+        def _():
+            arrived(1, p, near > 1)
 
     def project(half, index):
         rs = pl.multiple_of(half_start(half), 16)
@@ -218,15 +230,18 @@
     gate_inputs(0)
     y_kv(0).wait_recv()
     send_own(1)
+    arrived_near(0)
 
     tok_copy(tp2, tp2, 0).wait_recv()
     onward = tok_copy(tp2, tp1, 2)
     onward.start()
     tok_copy(tp3, tp1, 2).wait_recv()
     attention_inputs(1)
+    arrived_near(1)
     gate_inputs(1)
     y_kv(1).wait_recv()
     send_own(3)
+    arrived_near(2)
 
     mixed[...] = (gates[0].astype(F32) * gates[1].astype(F32)).astype(BF16)
     halo_copy = pltpu.make_async_remote_copy(
@@ -284,6 +299,44 @@
 
     attend(g, True)
 
+    arrived_near(3)
+
+    @pl.when(g > 0)
+    def _():
+        attend(g - 1, False)
+
+    def chain(d, carry):
+        for p in range(4):
+            arrived(d, p, d < near)
+        attend(g - d, False)
+        return carry
+
+    lax.fori_loop(2, g + 1, chain, 0)
+
+    gains = head_gain[...].astype(F32).reshape(1, 2 * HEAD)
+    gain = jnp.where(par == 0, gains[:, :HEAD], gains[:, HEAD:])
+
+    def finished(block, half):
+        rows = pl.ds(pl.multiple_of(block * R + half_start(half), 16), HR)
+        return rms(acc[rows, :] / total[rows, :], gain)
+
+    def back(half):
+        rows = pl.ds(half_start(half), HR)
+        return pltpu.make_async_remote_copy(
+            src_ref=ret.at[rows, :],
+            dst_ref=heads.at[par, rows, :],
+            send_sem=ret_send.at[half],
+            recv_sem=ret_recv.at[half],
+            device_id={"sp": mate},
+            device_id_type=MESH,
+        )
+
+    for half in (1, 0):
+        ret[pl.ds(pl.multiple_of(half_start(half), 16), HR), :] = finished(1 - par, half)
+        back(half).start()
+    for half in (1, 0):
+        heads[par, pl.ds(pl.multiple_of(half_start(half), 16), HR), :] = finished(par, half)
+
     @pl.when(sp > 0)
     def _():
         halo_copy.wait_recv()
@@ -298,43 +351,14 @@
     for j in range(KTAP):
         summed = summed + taps[j : j + 1, :].astype(F32) * padded[pl.ds(9 - KTAP + j, R), :]
     conv_out = gates[2].astype(F32) * summed
+    conv_gain = channel_gain[...].astype(F32).reshape(1, conv_out.shape[1])
     for h in range(conv_out.shape[1] // HEAD):
         cols = slice(h * HEAD, (h + 1) * HEAD)
-        group[:, cols] = rms(conv_out[:, cols], channel_gain[:, cols].astype(F32))
-
-    def chain(d, carry):
-        for p in range(4):
-            piece_copy(d - 1, p, 1, kv_send.at[0, p]).wait_recv()
-
-            @pl.when((d < near) & (g + 1 < G))
-            def _():
-                piece_copy(d, p, 1, kv_send.at[d, p]).start()
-
-        attend(g - d, False)
-        return carry
-
-    lax.fori_loop(1, g + 1, chain, 0)
-
-    gain = jnp.where(par == 0, head_gain[:, :HEAD], head_gain[:, HEAD:]).astype(F32)
-
-    def finished(first):
-        rows = pl.ds(pl.multiple_of(first, 16), R)
-        return rms(acc[rows, :] / total[rows, :], gain)
-
-    ret[...] = finished((1 - par) * R)
-    back = pltpu.make_async_remote_copy(
-        src_ref=ret,
-        dst_ref=heads.at[par],
-        send_sem=ret_send,
-        recv_sem=ret_recv,
-        device_id={"sp": mate},
-        device_id_type=MESH,
-    )
-    back.start()
-    heads[par] = finished(par * R)
+        group[:, cols] = rms(conv_out[:, cols], conv_gain[:, cols])
+
     for copy in wo_copies:
         copy.wait()
-    back.wait_recv()
+    back(1).wait_recv()
 
     NH = out.shape[1] // 2
 
@@ -374,6 +398,7 @@
         pair_copy(0, n).wait_recv()
         xsum[n] = (value + part_in[0, n].astype(F32)).astype(BF16)
         x_copy(n).start()
+    back(0).wait_recv()
     for n in range(2):
         part[1, n] = partial(tp1, n).astype(BF16)
         pair_copy(1, n).start()
@@ -390,7 +415,8 @@
     for half in range(2):
         y_kv(half).wait_send()
         y_q(half).wait_send()
-    back.wait_send()
+    back(0).wait_send()
+    back(1).wait_send()
 
     @pl.when(sp + 1 < S)
     def _():
@@ -468,8 +494,8 @@
             dma((G + 1, 4)),
             dma,
             dma,
-            dma,
-            dma,
+            dma((2,)),
+            dma((2,)),
             dma((2, 2)),
             dma((2, 2)),
             dma((2,)),
@@ -488,8 +514,8 @@
         wci,
         taps,
         gate,
-        head_gain.reshape(1, A),
-        channel_gain.reshape(1, A),
+        head_gain,
+        channel_gain,
         wattn,
         wchan,
     )

time: 60.3 us -> 57.4 us (0.952)
  local copies, waits for them, and re-layouts: 3.55 us -> 1.77 us
  Pallas kernels: 56.5 us -> 55.4 us
    reshape x2 -> x0, local copies, waits for them, and re-layouts: 1.77 us -> none  [the longest x1 1.23 us: local(): head_gain.reshape(1, A)]
    pallas_call x1, Pallas kernels: 56.5 us -> 55.4 us  [local(): pl.pallas_call(functools.partial(kernel, S, T), out_shape=jax.ShapeDtypeS...]
    unnamed x3 -> x1, local copies, waits for them, and re-layouts: 1.77 us -> 1.77 us
where the time goes in v2:
time: 57.4 us; the launch traced here: 57.2 us
  Pallas kernels  55.4 us (97%)
  local copies, waits for them, and re-layouts  1.77 us (3%)
    pallas_call x1, Pallas kernels, local(): pl.pallas_call(functools.partial(kernel, S, T), out_shape=jax.ShapeDtypeS...  55.4 us
    unnamed x1, local copies, waits for them, and re-layouts  1.77 us

profile of v2, /device:TPU:25, one launch (start us, length us, event | category | flops | bytes accessed | tf_op | source)
XLA Modules:
  0.0 57.2 jit_solution(1968934267122439905)
XLA Ops:
  0.0 55.4 %shard_map.127 = bf16[96,2048]{1,0:T(8,128)(2,1)} custom-call(bf16[96,2048]{1,0:T(8,128)(2,1)} %tokens.1, bf16[2048,256]{1,0:T(8,128)(2,1)} %wq.1, bf16[2048,256]{1,0:T(8,128)(2,1)} %wk.1, bf16[2048,256]{1,0:T(8,128)(2,1)} %wv.1, bf16[2048,256]{1,0:T(8,128)(2,1)} %wgo.1, bf16[2048,256]{1,0:T(8,128)(2,1)} %wgi.1, bf16[2048,256]{1,0:T(8,128)(2,1)} %wci.1, ...), custom_call_target="tpu_custom_call" | custom-call | tf_op jit(solution)/shard_map/pallas_call | solution.py:458
  55.4 1.8 %copy.15 = bf16[96,2048]{1,0:T(8,128)(2,1)} copy(bf16[96,2048]{1,0:T(8,128)(2,1)} %shard_map.127) | data formatting | bytes 786432

commit v3 on v2

--- a/solution.py
+++ b/solution.py
@@ -59,6 +59,8 @@
     part_in,
     xsum,
     xsum_in,
+    chan,
+    kept,
     w_sem,
     wo_sem,
     tok_sem,
@@ -67,7 +69,6 @@
     y_send,
     y_recv,
     kv_send,
-    kv_far,
     kv_recv,
     halo_send,
     halo_recv,
@@ -92,7 +93,8 @@
     tp1 = tp + 1 - 2 * (tp % 2)
     tp2 = (tp + 2) % T
     tp3 = (tp1 + 2) % T
-    near = G // 2
+    near = G - 1
+    forwards = g + 1 < G
 
     weights = (wk, wv, wq, wgi, wci, wgo)
     own_copy = pltpu.make_async_copy(tokens, tok.at[pl.ds(tp * C, C)], tok_sem)
@@ -173,12 +175,6 @@
         def _():
             piece_copy(0, p, 1, kv_send.at[0, p]).start()
 
-        for step in range(near + 1, G):
-
-            @pl.when(g + step < G)
-            def _():
-                piece_copy(0, p, step, kv_far.at[step, p]).start()
-
     def arrived(d, p, send_on):
         piece_copy(d, p, 0, kv_send.at[d, p]).wait_recv()
 
@@ -186,10 +182,22 @@
         def _():
             piece_copy(d, p, 1, kv_send.at[d, p]).start()
 
-    def arrived_near(p):
-        @pl.when(g > 0)
-        def _():
-            arrived(1, p, near > 1)
+    def early(d, p):
+        if d < near:
+
+            @pl.when((g >= d) & forwards)
+            def _():
+                arrived(d, p, True)
+
+    def late(d, p):
+        if d < near:
+
+            @pl.when(jnp.logical_not(forwards))
+            def _():
+                arrived(d, p, False)
+
+        else:
+            arrived(d, p, False)
 
     def project(half, index):
         rs = pl.multiple_of(half_start(half), 16)
@@ -230,18 +238,20 @@
     gate_inputs(0)
     y_kv(0).wait_recv()
     send_own(1)
-    arrived_near(0)
+    early(1, 0)
 
     tok_copy(tp2, tp2, 0).wait_recv()
     onward = tok_copy(tp2, tp1, 2)
     onward.start()
     tok_copy(tp3, tp1, 2).wait_recv()
     attention_inputs(1)
-    arrived_near(1)
+    early(1, 1)
     gate_inputs(1)
+    early(2, 0)
     y_kv(1).wait_recv()
     send_own(3)
-    arrived_near(2)
+    early(1, 2)
+    early(2, 1)
 
     mixed[...] = (gates[0].astype(F32) * gates[1].astype(F32)).astype(BF16)
     halo_copy = pltpu.make_async_remote_copy(
@@ -299,11 +309,22 @@
 
     attend(g, True)
 
-    arrived_near(3)
-
-    @pl.when(g > 0)
+    early(1, 3)
+    early(2, 2)
+
+    @pl.when(g >= 1)
     def _():
+        for p in range(4):
+            late(1, p)
         attend(g - 1, False)
+
+    early(2, 3)
+
+    @pl.when(g >= 2)
+    def _():
+        for p in range(4):
+            late(2, p)
+        attend(g - 2, False)
 
     def chain(d, carry):
         for p in range(4):
@@ -311,7 +332,7 @@
         attend(g - d, False)
         return carry
 
-    lax.fori_loop(2, g + 1, chain, 0)
+    lax.fori_loop(3, g + 1, chain, 0)
 
     gains = head_gain[...].astype(F32).reshape(1, 2 * HEAD)
     gain = jnp.where(par == 0, gains[:, :HEAD], gains[:, HEAD:])
@@ -358,17 +379,21 @@
 
     for copy in wo_copies:
         copy.wait()
+    NS = part.shape[1]
+    NH = out.shape[1] // NS
+    for n in range(NS):
+        cols = pl.ds(n * NH, NH)
+        chan[:, cols] = jnp.dot(group[...], wo[1, :, cols], preferred_element_type=F32)
     back(1).wait_recv()
 
-    NH = out.shape[1] // 2
-
-    def partial(chunk, n):
-        rows = pl.ds(pl.multiple_of(chunk * C, 16), C)
+    def partial(half, n):
+        rows = pl.ds(pl.multiple_of(half_start(half), 16), HR)
         both = jnp.concatenate([heads[0, rows, :], heads[1, rows, :]], axis=1)
         cols = pl.ds(n * NH, NH)
-        return jnp.dot(both, wo[0, :, cols], preferred_element_type=F32) + jnp.dot(
-            group[rows, :], wo[1, :, cols], preferred_element_type=F32
-        )
+        value = jnp.dot(both, wo[0, :, cols], preferred_element_type=F32) + chan[rows, cols]
+        a, b = value[:C], value[C:]
+        first = tp % 2 == 0
+        return jnp.where(first, a, b), jnp.where(first, b, a)
 
     def pair_copy(i, n):
         return pltpu.make_async_remote_copy(
@@ -390,24 +415,27 @@
             device_id_type=MESH,
         )
 
-    for n in range(2):
-        part[0, n] = partial(tp3, n).astype(BF16)
+    for n in range(NS):
+        mine, theirs = partial(1, n)
+        part[0, n] = theirs.astype(BF16)
         pair_copy(0, n).start()
-    for n in range(2):
-        value = partial(tp2, n)
+        kept[n] = mine
+    for n in range(NS):
         pair_copy(0, n).wait_recv()
-        xsum[n] = (value + part_in[0, n].astype(F32)).astype(BF16)
+        xsum[n] = (kept[n] + part_in[0, n].astype(F32)).astype(BF16)
         x_copy(n).start()
     back(0).wait_recv()
-    for n in range(2):
-        part[1, n] = partial(tp1, n).astype(BF16)
+    for n in range(NS):
+        mine, theirs = partial(0, n)
+        part[1, n] = theirs.astype(BF16)
         pair_copy(1, n).start()
-    for n in range(2):
-        value = partial(tp, n)
+        kept[n] = mine
+    for n in range(NS):
         pair_copy(1, n).wait_recv()
-        value = value + part_in[1, n].astype(F32)
+        kept[n] = kept[n] + part_in[1, n].astype(F32)
+    for n in range(NS):
         x_copy(n).wait_recv()
-        out[:, pl.ds(n * NH, NH)] = (value + xsum_in[n].astype(F32)).astype(BF16)
+        out[:, pl.ds(n * NH, NH)] = (kept[n] + xsum_in[n].astype(F32)).astype(BF16)
 
     cross.wait_send()
     beside.wait_send()
@@ -422,7 +450,7 @@
     def _():
         halo_copy.wait_send()
 
-    for n in range(2):
+    for n in range(NS):
         x_copy(n).wait_send()
         for i in range(2):
             pair_copy(i, n).wait_send()
@@ -437,12 +465,6 @@
             @pl.when((g + 1 < G) & (g >= d))
             def _():
                 piece_copy(d, p, 1, kv_send.at[d, p]).wait_send()
-
-        for step in range(near + 1, G):
-
-            @pl.when(g + step < G)
-            def _():
-                piece_copy(0, p, step, kv_far.at[step, p]).wait_send()
 
 
 def local(S, T, tokens, *rest):
@@ -452,12 +474,13 @@
     A = wq.shape[1]
     G = S // 2
     N = wattn.shape[1]
+    NS = 4
     hbm = pl.BlockSpec(memory_space=pl.ANY)
     vmem = pl.BlockSpec(memory_space=pltpu.VMEM)
     dma = pltpu.SemaphoreType.DMA
     return pl.pallas_call(
         functools.partial(kernel, S, T),
-        out_shape=jax.ShapeDtypeStruct((C, N), BF16),
+        out_shape=pltpu.VMEM((C, N), BF16),
         in_specs=[hbm] * 7 + [vmem] * 4 + [hbm] * 2,
         out_specs=vmem,
         scratch_shapes=[
@@ -478,10 +501,12 @@
             pltpu.VMEM((2 * R, HEAD), F32),
             pltpu.VMEM((R, HEAD), BF16),
             pltpu.VMEM((2, R, HEAD), BF16),
-            pltpu.VMEM((2, 2, C, N // 2), BF16),
-            pltpu.VMEM((2, 2, C, N // 2), BF16),
-            pltpu.VMEM((2, C, N // 2), BF16),
-            pltpu.VMEM((2, C, N // 2), BF16),
+            pltpu.VMEM((2, NS, C, N // NS), BF16),
+            pltpu.VMEM((2, NS, C, N // NS), BF16),
+            pltpu.VMEM((NS, C, N // NS), BF16),
+            pltpu.VMEM((NS, C, N // NS), BF16),
+            pltpu.VMEM((R, N), F32),
+            pltpu.VMEM((NS, C, N // NS), F32),
             dma((6,)),
             dma((2,)),
             dma,
@@ -491,15 +516,14 @@
             dma((2, 2)),
             dma((G, 4)),
             dma((G, 4)),
-            dma((G + 1, 4)),
             dma,
             dma,
             dma((2,)),
             dma((2,)),
-            dma((2, 2)),
-            dma((2, 2)),
-            dma((2,)),
-            dma((2,)),
+            dma((2, NS)),
+            dma((2, NS)),
+            dma((NS,)),
+            dma((NS,)),
         ],
         compiler_params=pltpu.CompilerParams(
             collective_id=0, has_side_effects=True, vmem_limit_bytes=60 * 1024 * 1024

time: 57.4 us -> 54.4 us (0.948)
  Pallas kernels: 55.4 us -> 53.5 us
  local copies, waits for them, and re-layouts: 1.77 us -> 0.75 us
    pallas_call x1, Pallas kernels: 55.4 us -> 53.5 us  [local(): pl.pallas_call(functools.partial(kernel, S, T), out_shape=pltpu.VMEM((C,...]
    unnamed x1, local copies, waits for them, and re-layouts: 1.77 us -> 0.75 us
where the time goes in v3:
time: 54.4 us; the launch traced here: 54.2 us
  Pallas kernels  53.5 us (98%)
  local copies, waits for them, and re-layouts  0.75 us (1%)
    pallas_call x1, Pallas kernels, local(): pl.pallas_call(functools.partial(kernel, S, T), out_shape=pltpu.VMEM((C,...  53.5 us

profile of v3, /device:TPU:25, one launch (start us, length us, event | category | flops | bytes accessed | tf_op | source)
XLA Modules:
  0.0 54.2 jit_solution(4120708937708432008)
XLA Ops:
  0.0 53.5 %shard_map.127 = bf16[96,2048]{1,0:T(8,128)(2,1)S(1)} custom-call(bf16[96,2048]{1,0:T(8,128)(2,1)} %tokens.1, bf16[2048,256]{1,0:T(8,128)(2,1)} %wq.1, bf16[2048,256]{1,0:T(8,128)(2,1)} %wk.1, bf16[2048,256]{1,0:T(8,128)(2,1)} %wv.1, bf16[2048,256]{1,0:T(8,128)(2,1)} %wgo.1, bf16[2048,256]{1,0:T(8,128)(2,1)} %wgi.1, bf16[2048,256]{1,0:T(8,128)(2,1)} %wci.1, ...), custom_call_target="tpu_custom_call" | custom-call | tf_op jit(solution)/shard_map/pallas_call | solution.py:481
  53.5 0.7 %copy.15 = bf16[96,2048]{1,0:T(8,128)(2,1)} copy(bf16[96,2048]{1,0:T(8,128)(2,1)S(1)} %shard_map.127) | data formatting | bytes 786432
